TPU v7x, 32 devices: a whole 2x2x4 slice. The times are simulated.
32 devices in a mesh: fs: 4 (over y, x), tp: 8 (over z, core).
Axes of the slice: x: 2, y: 2, z: 4, core: 2. Of those that a mesh axis runs over, the one named last changes fastest.
Arguments:
- tokens: bfloat16 [2048, 2048], P('fs', 'tp'), may hold values from -6 to 6
- norm_gain: float32 [2048], P('fs'), may hold values from 0.1 to 1.9
- gate_train: float32 [2048, 8192], P('fs', 'tp'), may hold values from -0.125 to 0.125
- up_train: float32 [2048, 8192], P('fs', 'tp'), may hold values from -0.125 to 0.125
- down_train: float32 [8192, 2048], P('fs', 'tp'), may hold values from -0.0625 to 0.0625
Outputs:
- gate_serve: bfloat16 [2048, 8192], P(None, 'tp')
- up_serve: bfloat16 [2048, 8192], P(None, 'tp')
- down_serve: bfloat16 [8192, 2048], P('tp')
- layer_out: bfloat16 [2048, 2048], P(('fs', 'tp'))
All inputs are finite; a program needn't handle non-finite values.
Results may differ from a plain program's by a relative error of at most 0.024.
Values may be sent and summed in bfloat16 or wider, within the bound.
A program may use at most 64 MiB of HBM per device.

v0:
```python
import jax
import jax.numpy as jnp
from jax import lax
from jax.sharding import PartitionSpec as P

D = 2048
epsilon = 1e-06


def body(tokens, norm_gain, gate_train, up_train, down_train):
    gate_local = (norm_gain[:, None] * gate_train).astype(jnp.bfloat16)
    up_local = (norm_gain[:, None] * up_train).astype(jnp.bfloat16)
    down_local = down_train.astype(jnp.bfloat16)
    features = lax.all_gather(tokens, "tp", axis=1, tiled=True)
    wide = features.astype(jnp.float32)
    squares = jnp.sum(wide * wide, axis=1)
    gate_whole, up_whole = (
        lax.all_gather(gate_local, "fs", axis=0, tiled=True),
        lax.all_gather(up_local, "fs", axis=0, tiled=True),
    )
    gate_sum = jnp.dot(features, gate_whole, preferred_element_type=jnp.float32)
    up_sum = jnp.dot(features, up_whole, preferred_element_type=jnp.float32)
    down_rows = lax.all_gather(down_local, "fs", axis=0, tiled=True)
    down_whole = lax.all_to_all(down_rows, "tp", split_axis=0, concat_axis=1, tiled=True)
    scale = lax.rsqrt(squares / D + epsilon)[:, None]
    hidden = (jax.nn.silu(gate_sum * scale) * (up_sum * scale)).astype(jnp.bfloat16)
    mixed = lax.psum_scatter(
        jnp.dot(hidden, down_whole, preferred_element_type=jnp.float32).astype(jnp.bfloat16),
        "tp",
        scatter_dimension=0,
        tiled=True,
    )
    return (gate_whole, up_whole, down_whole, mixed)


def solution(mesh):
    return jax.shard_map(
        body,
        mesh=mesh,
        in_specs=(P("fs", "tp"), P("fs"), P("fs", "tp"), P("fs", "tp"), P("fs", "tp")),
        out_specs=(P(None, "tp"), P(None, "tp"), P("tp", None), P(("fs", "tp"), None)),
        check_vma=False,
    )
```

profile of v0, /device:TPU:0, one launch (start us, length us, event | category | flops | bytes accessed | tf_op | source)
XLA Modules:
  0.0 293.7 jit_solution(2137613969868247611)
XLA Ops:
  7.2 0.0 copy-start.2
  7.2 0.0 copy-start.3
  7.2 0.0 all-gather.9.cloned.1.call-start
  7.2 2.8 convert_element_type.20
  10.0 0.0 all-gather.9.cloned.1.call-update
  10.1 0.0 all-gather.11.cloned.1.call-start
  10.1 0.7 all-gather.11.cloned.1.call-update
  10.8 0.0 all-gather.5.cloned.1.call-start
  10.9 0.0 copy-done.2
  10.9 0.0 copy-done.3
  10.9 3.2 %multiply_convert_fusion = (bf16[512,1024]{1,0:T(8,128)(2,1)}, bf16[512,1024]{1,0:T(8,128)(2,1)}) fusion(f32[512,1024]{1,0:T(8,128)S(1)} %copy-done.2, f32[512]{0:T(512)S(1)} %copy-done.3, f32[512,1024]{1,0:T(8,128)} %param.7), kind=kLoop, calls=%fused_computation.9 | loop fusion | flops 2097152 | bytes 6293504 | tf_op jit(solution)/shard_map/convert_element_type | solution.py:12
  14.1 0.0 all-gather.5.cloned.1.call-update
  14.1 51.6 %all-gather.9.cloned.1.call-done = bf16[8192,256]{1,0:T(8,128)(2,1)} async-done(((bf16[2048,256]{1,0:T(8,128)(2,1)}), bf16[8192,256]{1,0:T(8,128)(2,1)}) %all-gather.9.cloned.1.call-update) | async-done | bytes 4194320 | tf_op jit(solution)/shard_map/all_gather | solution.py:23
  65.7 4.6 %all-to-all-start = ((bf16[8,1024,256]{2,1,0:T(8,128)(2,1)}), bf16[8,1024,256]{2,1,0:T(8,128)(2,1)}, u32[]{:S(2)}, u32[]{:S(2)}) async-start(bf16[8,1024,256]{2,1,0:T(8,128)(2,1)} %bitcast.32), calls=%async_computation | async-start | bytes 8388608 | tf_op jit(solution)/shard_map/all_to_all | solution.py:24
  70.3 0.0 all-gather.7.cloned.1.call-start
  70.4 0.5 all-gather.7.cloned.1.call-update
  70.9 0.0 reduce-scatter.2.cloned.1.call-start
  71.0 50.9 %all-gather.11.cloned.1.call-done = bf16[512,2048]{1,0:T(8,128)(2,1)} async-done(((bf16[512,256]{1,0:T(8,128)(2,1)}), bf16[512,2048]{1,0:T(8,128)(2,1)}) %all-gather.11.cloned.1.call-update) | async-done | bytes 2097168 | tf_op jit(solution)/shard_map/all_gather | solution.py:14
  121.8 2.2 multiply_reduce_fusion
  124.1 54.8 %all-gather.5.cloned.1.call-done = bf16[2048,1024]{1,0:T(8,128)(2,1)} async-done(((bf16[512,1024]{1,0:T(8,128)(2,1)}), bf16[2048,1024]{1,0:T(8,128)(2,1)}) %all-gather.5.cloned.1.call-update) | async-done | bytes 4194320 | tf_op jit(solution)/shard_map/all_gather | solution.py:18
  178.9 0.0 copy-done.1
  178.9 5.9 %fusion.5 = f32[1024,512]{1,0:T(8,128)} fusion(bf16[2048,1024]{1,0:T(8,128)(2,1)} %all-gather.5.cloned.1.call-done, bf16[512,2048]{1,0:T(8,128)(2,1)S(1)} %copy-done.1), kind=kOutput, calls=%fused_computation.13 | convolution fusion | flops 2147483648 | bytes 8388608 | tf_op jit(solution)/shard_map/dot_general | solution.py:21
  184.8 0.0 all-to-all-done
  184.8 6.5 %copy.10 = bf16[8,1024,256]{1,2,0:T(8,128)(2,1)} copy(bf16[8,1024,256]{2,1,0:T(8,128)(2,1)} %all-to-all-done) | data formatting | bytes 8388608 | tf_op jit(solution)/shard_map/all_to_all | solution.py:24
  191.2 42.5 %all-gather.7.cloned.1.call-done = bf16[2048,1024]{1,0:T(8,128)(2,1)} async-done(((bf16[512,1024]{1,0:T(8,128)(2,1)}), bf16[2048,1024]{1,0:T(8,128)(2,1)}) %all-gather.7.cloned.1.call-update) | async-done | bytes 4194320 | tf_op jit(solution)/shard_map/all_gather | solution.py:19
  233.7 10.3 %convolution_convert_fusion = bf16[512,2048]{1,0:T(8,128)(2,1)} fusion(bf16[1024,2048]{0,1:T(8,128)(2,1)} %bitcast.30, f32[1024,512]{1,0:T(8,128)} %fusion.5, bf16[2048,1024]{1,0:T(8,128)(2,1)} %all-gather.7.cloned.1.call-done, bf16[512,2048]{1,0:T(8,128)(2,1)S(1)} %copy-done.1, f32[512]{0:T(512)S(1)} %add_rsqrt_fusion), kind=kOutput, calls=%fused_computation.1 | convolution fusion | flops 4300210176 | bytes 14682112 | tf_op jit(solution)/shard_map/dot_general | solution.py:28
  244.0 0.0 reduce-scatter.2.cloned.1.call-update
  244.0 6.4 %copy.11 = bf16[1024,2048]{1,0:T(8,128)(2,1)} copy(bf16[1024,2048]{0,1:T(8,128)(2,1)} %bitcast.31) | data formatting | bytes 8388608
  250.5 29.8 %reduce-scatter.2.cloned.1.call-done = bf16[64,2048]{1,0:T(8,128)(2,1)} async-done(((bf16[512,2048]{1,0:T(8,128)(2,1)}), bf16[64,2048]{1,0:T(8,128)(2,1)}) %reduce-scatter.2.cloned.1.call-update) | async-done | bytes 262160 | tf_op jit(solution)/shard_map/reduce_scatter | solution.py:27
  280.3 4.8 %copy.14 = bf16[2048,1024]{1,0:T(8,128)(2,1)} copy(bf16[2048,1024]{1,0:T(8,128)(2,1)} %all-gather.5.cloned.1.call-done) | data formatting | bytes 8388608
  285.1 0.0 copy-done
  285.1 2.0 copy.15
  (3 shorter events, 0.0 us)
Async XLA Ops:
  7.2 3.7 %copy-start.2 = (f32[512,1024]{1,0:T(8,128)S(1)}, f32[512,1024]{1,0:T(8,128)}, u32[]{:S(2)}) copy-start(f32[512,1024]{1,0:T(8,128)} %param.8) | copy-start | bytes 6291460
  7.2 3.7 %copy-start.3 = (f32[512]{0:T(512)S(1)}, f32[512]{0:T(512)}, u32[]{:S(2)}) copy-start(f32[512]{0:T(512)} %param.6) | copy-start | bytes 6148
  7.2 58.6 %all-gather.9.cloned.1.call-start = ((), (), s32[]{:S(2)}) async-start(), calls=%async_computation.4 | async-start | bytes 5242880 | tf_op jit(solution)/shard_map/all_gather | solution.py:23
  10.1 111.8 %all-gather.11.cloned.1.call-start = ((), (), s32[]{:S(2)}) async-start(), calls=%async_computation.5 | async-start | bytes 2359296 | tf_op jit(solution)/shard_map/all_gather | solution.py:14
  10.8 168.1 %all-gather.5.cloned.1.call-start = ((), (), s32[]{:S(2)}) async-start(), calls=%async_computation.2 | async-start | bytes 5242880 | tf_op jit(solution)/shard_map/all_gather | solution.py:18
  65.7 119.0 %all-to-all-start = ((bf16[8,1024,256]{2,1,0:T(8,128)(2,1)}), bf16[8,1024,256]{2,1,0:T(8,128)(2,1)}, u32[]{:S(2)}, u32[]{:S(2)}) async-start(bf16[8,1024,256]{2,1,0:T(8,128)(2,1)} %bitcast.32), calls=%async_computation | async-start | bytes 8388608 | tf_op jit(solution)/shard_map/all_to_all | solution.py:24
  70.3 163.4 %all-gather.7.cloned.1.call-start = ((), (), s32[]{:S(2)}) async-start(), calls=%async_computation.3 | async-start | bytes 5242880 | tf_op jit(solution)/shard_map/all_gather | solution.py:19
  70.9 209.4 %reduce-scatter.2.cloned.1.call-start = ((), (), s32[]{:S(2)}) async-start(), calls=%async_computation.6 | async-start | bytes 2359296 | tf_op jit(solution)/shard_map/reduce_scatter | solution.py:27
  121.8 57.0 %copy-start.1 = (bf16[512,2048]{1,0:T(8,128)(2,1)S(1)}, bf16[512,2048]{1,0:T(8,128)(2,1)}, u32[]{:S(2)}) copy-start(bf16[512,2048]{1,0:T(8,128)(2,1)} %all-gather.11.cloned.1.call-done) | copy-start | bytes 6291460
  280.3 4.8 %copy-start = (bf16[2048,1024]{1,0:T(8,128)(2,1)S(1)}, bf16[2048,1024]{1,0:T(8,128)(2,1)}, u32[]{:S(2)}) copy-start(bf16[2048,1024]{1,0:T(8,128)(2,1)} %all-gather.7.cloned.1.call-done) | copy-start | bytes 12582916
Sparse Core Ops, SparseCore 0:
  10.4 55.2 all-gather.8
  67.3 54.4 all-gather.10
  124.3 54.5 all-gather.4
  181.1 52.5 all-gather.6
  244.2 36.0 reduce-scatter.1
where the time goes:
time: 294 us
  waiting for transfers between devices  231 us (79%)
  local copies, waits for them, and re-layouts  19.8 us (7%)
  matrix products  16.2 us (6%)
  between operations  13.8 us (5%)
  other arithmetic  8.23 us (3%)
  starting transfers between devices  4.8 us (2%)
    all_gather x1, waiting for transfers between devices, body(): lax.all_gather(gate_local, 'fs', axis=0, tiled=True)  54.8 us
    all_gather x1, waiting for transfers between devices, body(): down_rows = lax.all_gather(down_local, 'fs', axis=0, tiled=True)  51.6 us
    all_gather x1, waiting for transfers between devices, body(): features = lax.all_gather(tokens, 'tp', axis=1, tiled=True)  50.9 us
    all_gather x1, waiting for transfers between devices, body(): lax.all_gather(up_local, 'fs', axis=0, tiled=True)  42.5 us
    reduce_scatter x1, waiting for transfers between devices, body(): lax.psum_scatter(jnp.dot(hidden, down_whole, preferred_element_type=jnp.f...  29.8 us
    unnamed x11, local copies, waits for them, and re-layouts  13.3 us
    dot_general x1, matrix products, body(): jnp.dot(hidden, down_whole, preferred_element_type=jnp.float32)  10.3 us
    all_to_all x1, local copies, waits for them, and re-layouts, body(): lax.all_to_all(down_rows, 'tp', split_axis=0, concat_axis=1, tiled=True)  6.48 us
  transfers between devices with their start and end apart: 6, of which 5 were waited for; matrix products, arithmetic and copies ran while one was open for 8% of the time, Pallas kernels for 0%

commit v1 on v0

--- a/solution.py
+++ b/solution.py
@@ -20,7 +20,21 @@
     )
     gate_sum = jnp.dot(features, gate_whole, preferred_element_type=jnp.float32)
     up_sum = jnp.dot(features, up_whole, preferred_element_type=jnp.float32)
-    down_rows = lax.all_gather(down_local, "fs", axis=0, tiled=True)
+
+    def apply_lines(vec, along_axis, k_dim):
+        many = lax.psum(1, along_axis)
+        grid = [vec]
+        for nth in range(many - 1):
+            passed = lax.ppermute(grid[-1], along_axis, [(t, (t + 1) % many) for t in range(many)])
+            grid.append(passed)
+        carry_in = jnp.roll(
+            jnp.concatenate(grid[::-1], k_dim),
+            (lax.axis_index(along_axis) + 1) * vec.shape[k_dim],
+            k_dim,
+        )
+        return carry_in
+
+    down_rows = apply_lines(down_local, "fs", 0)
     down_whole = lax.all_to_all(down_rows, "tp", split_axis=0, concat_axis=1, tiled=True)
     scale = lax.rsqrt(squares / D + epsilon)[:, None]
     hidden = (jax.nn.silu(gate_sum * scale) * (up_sum * scale)).astype(jnp.bfloat16)

time: 294 us -> 285 us (0.969)
  waiting for transfers between devices: 231 us -> 208 us
  local copies, waits for them, and re-layouts: 19.8 us -> 27.5 us
  starting transfers between devices: 4.8 us -> 10.4 us
    ppermute x0 -> x3, waiting for transfers between devices: none -> 92.5 us  [apply_lines(): lax.ppermute(grid[-1], along_axis, [(t, (t + 1) % many) for t in range(ma...]
    all_to_all x1, waiting for transfers between devices: 0.01 us -> 84.6 us  [body(): lax.all_to_all(down_rows, 'tp', split_axis=0, concat_axis=1, tiled=True)]
    all_gather x1, waiting for transfers between devices: 54.8 us -> 0.02 us  [body(): lax.all_gather(gate_local, 'fs', axis=0, tiled=True)]
    all_gather x1 -> x0, waiting for transfers between devices: 51.6 us -> none  [body(): down_rows = lax.all_gather(down_local, 'fs', axis=0, tiled=True)]
    all_gather x1, waiting for transfers between devices: 50.9 us -> 0.02 us  [body(): features = lax.all_gather(tokens, 'tp', axis=1, tiled=True)]
    all_gather x1, waiting for transfers between devices: 42.5 us -> 0.01 us  [body(): lax.all_gather(up_local, 'fs', axis=0, tiled=True)]
    unnamed x11 -> x17, local copies, waits for them, and re-layouts: 13.3 us -> 18.6 us
    ppermute x0 -> x3, starting transfers between devices: none -> 4.64 us  [apply_lines(): lax.ppermute(grid[-1], along_axis, [(t, (t + 1) % many) for t in range(ma...]
  transfers between devices with their start and end apart: 6 -> 8, of which waited for: 5 -> 5; matrix products, arithmetic and copies ran while one was open for 8% -> 12% of each run, Pallas kernels for 0% -> 0%
where the time goes in v1:
time: 285 us; the launch traced here: 284 us
  waiting for transfers between devices  208 us (73%)
  local copies, waits for them, and re-layouts  27.5 us (10%)
  matrix products  16.9 us (6%)
  between operations  13.9 us (5%)
  starting transfers between devices  10.4 us (4%)
  other arithmetic  7.21 us (3%)
    ppermute x3, waiting for transfers between devices, apply_lines(): lax.ppermute(grid[-1], along_axis, [(t, (t + 1) % many) for t in range(ma...  92.5 us
    all_to_all x1, waiting for transfers between devices, body(): lax.all_to_all(down_rows, 'tp', split_axis=0, concat_axis=1, tiled=True)  84.6 us
    reduce_scatter x1, waiting for transfers between devices, body(): lax.psum_scatter(jnp.dot(hidden, down_whole, preferred_element_type=jnp.f...  29.7 us
    unnamed x17, local copies, waits for them, and re-layouts  18.6 us
    dot_general x1, matrix products, body(): jnp.dot(hidden, down_whole, preferred_element_type=jnp.float32)  10.3 us
    all_to_all x1, local copies, waits for them, and re-layouts, body(): lax.all_to_all(down_rows, 'tp', split_axis=0, concat_axis=1, tiled=True)  6.57 us
    dot_general x1, matrix products, body(): gate_sum = jnp.dot(features, gate_whole, preferred_element_type=jnp.float32)  6.57 us
  transfers between devices with their start and end apart: 8, of which 5 were waited for; matrix products, arithmetic and copies ran while one was open for 12% of the time, Pallas kernels for 0%

profile of v1, /device:TPU:0, one launch (start us, length us, event | category | flops | bytes accessed | tf_op | source)
XLA Modules:
  0.0 283.9 jit_solution(17187609945986158144)
XLA Ops:
  7.2 0.0 all-gather.8.cloned.1.call-start
  7.2 0.7 all-gather.8.cloned.1.call-update
  7.9 0.0 all-gather.4.cloned.1.call-start
  8.0 1.7 convert_element_type.20
  9.7 3.0 %collective-permute-start = (bf16[2048,256]{1,0:T(8,128)(2,1)S(1)}, bf16[2048,256]{1,0:T(8,128)(2,1)S(1)}, u32[]{:S(2)}, u32[]{:S(2)}) collective-permute-start(bf16[2048,256]{1,0:T(8,128)(2,1)S(1)} %convert_element_type.20), channel_id=1, source_target_pairs={{0,8},{8,16},{16,24},{24,0},{1,9},{9,17},{17,25},{25,1},{2,10},{10... | collective-permute-start | bytes 3145736 | tf_op jit(solution)/shard_map/ppermute | solution.py:28
  12.7 24.1 %collective-permute-done = bf16[2048,256]{1,0:T(8,128)(2,1)S(1)} collective-permute-done((bf16[2048,256]{1,0:T(8,128)(2,1)S(1)}, bf16[2048,256]{1,0:T(8,128)(2,1)S(1)}, u32[]{:S(2)}, u32[]{:S(2)}) %collective-permute-start) | collective-permute-done | bytes 1048608 | tf_op jit(solution)/shard_map/ppermute | solution.py:28
  36.8 0.8 collective-permute-start.1
  37.6 3.2 %multiply_convert_fusion = (bf16[512,1024]{1,0:T(8,128)(2,1)}, bf16[512,1024]{1,0:T(8,128)(2,1)}) fusion(f32[512,1024]{1,0:T(8,128)S(1)} %copy-done.3, f32[512]{0:T(512)} %param.6, f32[512,1024]{1,0:T(8,128)} %param.7), kind=kLoop, calls=%fused_computation.9 | loop fusion | flops 2097152 | bytes 6293504 | tf_op jit(solution)/shard_map/convert_element_type | solution.py:12
  40.8 29.7 %collective-permute-done.1 = bf16[2048,256]{1,0:T(8,128)(2,1)} collective-permute-done((bf16[2048,256]{1,0:T(8,128)(2,1)S(1)}, bf16[2048,256]{1,0:T(8,128)(2,1)}, u32[]{:S(2)}, u32[]{:S(2)}) %collective-permute-start.1) | collective-permute-done | bytes 1048608 | tf_op jit(solution)/shard_map/ppermute | solution.py:28
  70.5 0.8 collective-permute-start.2
  71.4 38.7 %collective-permute-done.2 = bf16[2048,256]{1,0:T(8,128)(2,1)} collective-permute-done((bf16[2048,256]{1,0:T(8,128)(2,1)}, bf16[2048,256]{1,0:T(8,128)(2,1)}, u32[]{:S(2)}, u32[]{:S(2)}) %collective-permute-start.2) | collective-permute-done | bytes 1048608 | tf_op jit(solution)/shard_map/ppermute | solution.py:28
  110.0 1.3 constant_dynamic-update-slice_fusion.7
  111.3 1.3 constant_dynamic-update-slice_fusion.6
  112.6 0.1 constant_dynamic-update-slice_fusion.5
  112.7 0.1 constant_dynamic-update-slice_fusion.4
  112.8 1.3 constant_dynamic-update-slice_fusion.3
  114.1 1.3 constant_dynamic-update-slice_fusion.2
  115.4 0.1 constant_dynamic-update-slice_fusion.1
  115.5 0.1 constant_dynamic-update-slice_fusion
  115.6 2.3 constant_dynamic-slice_fusion
  117.9 5.6 %all-to-all-start = ((bf16[8,1024,256]{2,1,0:T(8,128)(2,1)}), bf16[8,1024,256]{2,1,0:T(8,128)(2,1)}, u32[]{:S(2)}, u32[]{:S(2)}) async-start(bf16[8,1024,256]{2,1,0:T(8,128)(2,1)} %bitcast.29), calls=%async_computation | async-start | bytes 8388608 | tf_op jit(solution)/shard_map/all_to_all | solution.py:38
  123.5 0.7 all-gather.6.cloned.1.call-update
  124.2 0.0 reduce-scatter.2.cloned.1.call-start
  124.3 2.1 multiply_reduce_fusion
  126.4 6.6 %fusion.5 = f32[1024,512]{1,0:T(8,128)} fusion(bf16[2048,1024]{1,0:T(8,128)(2,1)} %all-gather.4.cloned.1.call-done, bf16[512,2048]{1,0:T(8,128)(2,1)} %all-gather.8.cloned.1.call-done), kind=kOutput, calls=%fused_computation.22 | convolution fusion | flops 2147483648 | bytes 8388608 | tf_op jit(solution)/shard_map/dot_general | solution.py:21
  132.9 84.6 %all-to-all-done = bf16[8,1024,256]{2,1,0:T(8,128)(2,1)} async-done(((bf16[8,1024,256]{2,1,0:T(8,128)(2,1)}), bf16[8,1024,256]{2,1,0:T(8,128)(2,1)}, u32[]{:S(2)}, u32[]{:S(2)}) %all-to-all-start) | async-done | bytes 4194336 | tf_op jit(solution)/shard_map/all_to_all | solution.py:38
  217.5 6.6 %copy.9 = bf16[1024,8,256]{0,2,1:T(8,128)(2,1)} copy(bf16[1024,8,256]{2,0,1:T(8,128)(2,1)} %bitcast.1) | data formatting | bytes 8388608 | tf_op jit(solution)/shard_map/all_to_all | solution.py:38
  224.1 10.3 %convolution_convert_fusion = bf16[512,2048]{1,0:T(8,128)(2,1)} fusion(bf16[1024,2048]{0,1:T(8,128)(2,1)} %bitcast.30, f32[1024,512]{1,0:T(8,128)} %fusion.5, bf16[2048,1024]{1,0:T(8,128)(2,1)} %all-gather.6.cloned.1.call-done, bf16[512,2048]{1,0:T(8,128)(2,1)S(1)} %copy-done.2, f32[512]{0:T(512)S(1)} %add_rsqrt_fusion), kind=kOutput, calls=%fused_computation.1 | convolution fusion | flops 4300210176 | bytes 14682112 | tf_op jit(solution)/shard_map/dot_general | solution.py:42
  234.5 6.4 %copy.10 = bf16[1024,2048]{1,0:T(8,128)(2,1)} copy(bf16[1024,2048]{0,1:T(8,128)(2,1)} %bitcast.31) | data formatting | bytes 8388608
  240.9 29.7 %reduce-scatter.2.cloned.1.call-done = bf16[64,2048]{1,0:T(8,128)(2,1)} async-done(((bf16[512,2048]{1,0:T(8,128)(2,1)}), bf16[64,2048]{1,0:T(8,128)(2,1)}) %reduce-scatter.2.cloned.1.call-update) | async-done | bytes 262160 | tf_op jit(solution)/shard_map/reduce_scatter | solution.py:41
  270.6 4.8 %copy.20 = bf16[2048,1024]{1,0:T(8,128)(2,1)} copy(bf16[2048,1024]{1,0:T(8,128)(2,1)} %all-gather.4.cloned.1.call-done) | data formatting | bytes 8388608
  275.4 2.0 copy.21
  (15 shorter events, 0.1 us)
Async XLA Ops:
  7.2 30.4 %copy-start.3 = (f32[512,1024]{1,0:T(8,128)S(1)}, f32[512,1024]{1,0:T(8,128)}, u32[]{:S(2)}) copy-start(f32[512,1024]{1,0:T(8,128)} %param.8) | copy-start | bytes 6291460
  7.2 117.1 %all-gather.8.cloned.1.call-start = ((), (), s32[]{:S(2)}) async-start(), calls=%async_computation.4 | async-start | bytes 2359296 | tf_op jit(solution)/shard_map/all_gather | solution.py:14
  7.9 118.5 %all-gather.4.cloned.1.call-start = ((), (), s32[]{:S(2)}) async-start(), calls=%async_computation.2 | async-start | bytes 5242880 | tf_op jit(solution)/shard_map/all_gather | solution.py:18
  9.7 27.1 %collective-permute-start = (bf16[2048,256]{1,0:T(8,128)(2,1)S(1)}, bf16[2048,256]{1,0:T(8,128)(2,1)S(1)}, u32[]{:S(2)}, u32[]{:S(2)}) collective-permute-start(bf16[2048,256]{1,0:T(8,128)(2,1)S(1)} %convert_element_type.20), channel_id=1, source_target_pairs={{0,8},{8,16},{16,24},{24,0},{1,9},{9,17},{17,25},{25,1},{2,10},{10... | collective-permute-start | bytes 3145736 | tf_op jit(solution)/shard_map/ppermute | solution.py:28
  36.8 33.7 %collective-permute-start.1 = (bf16[2048,256]{1,0:T(8,128)(2,1)S(1)}, bf16[2048,256]{1,0:T(8,128)(2,1)}, u32[]{:S(2)}, u32[]{:S(2)}) collective-permute-start(bf16[2048,256]{1,0:T(8,128)(2,1)S(1)} %collective-permute-done), channel_id=1, source_target_pairs={{0,8},{8,16},{16,24},{24,0},{1,9},{9,17},{17,25},{25,1},{2,10},{10... | collective-permute-start | bytes 3145736 | tf_op jit(solution)/shard_map/ppermute | solution.py:28
  40.8 71.9 %copy-start = (f32[2048,256]{1,0:T(8,128)S(1)}, f32[2048,256]{1,0:T(8,128)}, u32[]{:S(2)}) copy-start(f32[2048,256]{1,0:T(8,128)} %param.9) | copy-start | bytes 6291460
  70.5 39.5 %collective-permute-start.2 = (bf16[2048,256]{1,0:T(8,128)(2,1)}, bf16[2048,256]{1,0:T(8,128)(2,1)}, u32[]{:S(2)}, u32[]{:S(2)}) collective-permute-start(bf16[2048,256]{1,0:T(8,128)(2,1)} %collective-permute-done.1), channel_id=1, source_target_pairs={{0,8},{8,16},{16,24},{24,0},{1,9},{9,17},{17,25},{25,1},{2,10},{10... | collective-permute-start | bytes 3145736 | tf_op jit(solution)/shard_map/ppermute | solution.py:28
  117.9 99.6 %all-to-all-start = ((bf16[8,1024,256]{2,1,0:T(8,128)(2,1)}), bf16[8,1024,256]{2,1,0:T(8,128)(2,1)}, u32[]{:S(2)}, u32[]{:S(2)}) async-start(bf16[8,1024,256]{2,1,0:T(8,128)(2,1)} %bitcast.29), calls=%async_computation | async-start | bytes 8388608 | tf_op jit(solution)/shard_map/all_to_all | solution.py:38
  123.5 100.7 %all-gather.6.cloned.1.call-start = ((), (), s32[]{:S(2)}) async-start(), calls=%async_computation.3 | async-start | bytes 5242880 | tf_op jit(solution)/shard_map/all_gather | solution.py:19
  124.2 146.4 %reduce-scatter.2.cloned.1.call-start = ((), (), s32[]{:S(2)}) async-start(), calls=%async_computation.5 | async-start | bytes 2359296 | tf_op jit(solution)/shard_map/reduce_scatter | solution.py:41
  217.5 6.6 %copy-start.2 = (bf16[512,2048]{1,0:T(8,128)(2,1)S(1)}, bf16[512,2048]{1,0:T(8,128)(2,1)}, u32[]{:S(2)}) copy-start(bf16[512,2048]{1,0:T(8,128)(2,1)} %all-gather.8.cloned.1.call-done) | copy-start | bytes 6291460
  270.6 4.8 %copy-start.1 = (bf16[2048,1024]{1,0:T(8,128)(2,1)S(1)}, bf16[2048,1024]{1,0:T(8,128)(2,1)}, u32[]{:S(2)}) copy-start(bf16[2048,1024]{1,0:T(8,128)(2,1)} %all-gather.6.cloned.1.call-done) | copy-start | bytes 12582916
Sparse Core Ops, SparseCore 0:
  9.6 33.3 all-gather.7
  45.4 73.1 all-gather.3
  126.1 55.0 all-gather.5
  234.6 35.9 reduce-scatter.1
